TPU v7x, 32 devices: a whole 2x2x4 slice. The times are simulated.
32 devices in a mesh: ep: 16 (over z, y, x), tp: 2 (over core).
Axes of the slice: x: 2, y: 2, z: 4, core: 2. Of those that a mesh axis runs over, the one named last changes fastest.
Arguments:
- tokens: bfloat16 [384, 2048], P('ep'), may hold values from -6 to 6
- attn_gain: float32 [2048], replicated, may hold values from 0.1 to 1.9
- w_query: bfloat16 [2048, 1024], P(None, 'tp'), may hold values from -0.125 to 0.125
- w_key: bfloat16 [2048, 1024], P(None, 'tp'), may hold values from -0.125 to 0.125
- w_value: bfloat16 [2048, 1024], P(None, 'tp'), may hold values from -0.125 to 0.125
- w_zgate: bfloat16 [2048, 1024], P(None, 'tp'), may hold values from -0.125 to 0.125
- w_decay: bfloat16 [2048, 8], P(None, 'tp'), may hold values from -0.125 to 0.125
- w_beta: bfloat16 [2048, 8], P(None, 'tp'), may hold values from -0.125 to 0.125
- decay_rate: float32 [8], P('tp'), may hold values from 0.05 to 2
- decay_bias: float32 [8], P('tp'), may hold values from -3 to 3
- state: float32 [384, 8, 128, 128], P('ep', 'tp'), may hold values from -2 to 2
- out_gain: float32 [128], replicated, may hold values from 0.1 to 1.9
- w_out: bfloat16 [1024, 2048], P('tp'), may hold values from -0.1875 to 0.1875
- ffn_gain: float32 [2048], replicated, may hold values from 0.1 to 1.9
- expert_gate: bfloat16 [16, 2048, 512], P('ep', None, 'tp'), may hold values from -0.125 to 0.125
- expert_up: bfloat16 [16, 2048, 512], P('ep', None, 'tp'), may hold values from -0.125 to 0.125
- expert_down: bfloat16 [16, 512, 2048], P('ep', 'tp'), may hold values from -0.25 to 0.25
- routes: int32 [384, 2], P('ep'), may hold values from 0 to 15, all different within a row; in each aligned block of 24 rows (0 to 23, 24 to 47, ...) at most 6 rows name the same one
- route_weight: float32 [384, 2], P('ep'), may hold values from 0.2 to 1
Outputs:
- layer_out: bfloat16 [384, 2048], P('ep', 'tp')
- new_state: float32 [384, 8, 128, 128], P('ep', 'tp')
Inputs may be any that keep to these rules, and one draw needn't show every extreme that they name: `routes`: the 2 entries of a row differ. Among the rows of one index of ep (aligned blocks of 24 rows) no expert is named more than 6 times, a bound that some block reaches.
All inputs are finite; a program needn't handle non-finite values.
Results may differ from a plain program's by a relative error of at most 0.014.
Values may be sent and summed in bfloat16 or wider, within the bound.
A program may use at most 128 MiB of HBM per device.

v0:
```python
import functools

import jax
import jax.numpy as jnp
from jax import lax
from jax.experimental import pallas as pl
from jax.experimental.pallas import tpu as pltpu
from jax.sharding import PartitionSpec as P

EPS = 1e-06
F32 = jnp.float32
BF16 = jnp.bfloat16
VMEM_LIMIT = 60 * 1024 * 1024
HBM = pl.BlockSpec(memory_space=pltpu.HBM)
VMEM = pl.BlockSpec(memory_space=pltpu.VMEM)


def rms_scale(rows, gain):
    return rows * lax.rsqrt(jnp.mean(rows * rows, axis=-1, keepdims=True) + EPS) * gain


def unit_rows(rows):
    return rows * lax.rsqrt(jnp.sum(rows * rows, axis=-1, keepdims=True) + EPS)


def silu(x):
    return x * jax.nn.sigmoid(x)


def nt_dot(rows, weight):
    return lax.dot_general(rows, weight, (((1,), (1,)), ((), ())), preferred_element_type=F32)


def mixer_kernel(
    step,
    tokens_ref,
    gain_ref,
    wq,
    wk,
    wv,
    wz,
    wd_ref,
    wb_ref,
    rate_ref,
    bias_ref,
    state,
    out_gain_ref,
    heads_out,
    new_state,
    tokens,
    gain,
    wd,
    wb,
    rate,
    bias,
    out_gain,
    small_sem,
    wbuf,
    st,
    ns,
    kq,
    vals,
    zbuf,
    fades,
    betas,
    dots,
    reads,
    w_sem,
    in_sem,
    out_sem,
):
    seqs, heads, dim, _ = st.shape
    chunks = seqs // step

    def w_copy(n):
        return pltpu.make_async_copy((wq, wk, wv, wz)[n], wbuf.at[n], w_sem.at[n])

    def in_copy(c):
        rows = pl.ds(c * step, step)
        return pltpu.make_async_copy(state.at[rows], st.at[rows], in_sem.at[c])

    def out_copy(c):
        rows = pl.ds(c * step, step)
        return pltpu.make_async_copy(ns.at[rows], new_state.at[rows], out_sem.at[c])

    small = [
        pltpu.make_async_copy(src, dst, small_sem.at[n])
        for n, (src, dst) in enumerate(
            (
                (tokens_ref, tokens),
                (gain_ref, gain),
                (wd_ref, wd),
                (wb_ref, wb),
                (rate_ref, rate),
                (bias_ref, bias),
                (out_gain_ref, out_gain),
            )
        )
    ]
    for copy in small:
        copy.start()
    for n in range(4):
        w_copy(n).start()
    for c in range(chunks):
        in_copy(c).start()
    for copy in small:
        copy.wait()

    normed = rms_scale(tokens[...].astype(F32), gain[...]).astype(BF16)

    def rounded(weight):
        return jnp.dot(normed, weight, preferred_element_type=F32).astype(BF16).astype(F32)

    xa = nt_dot(normed, wd[...]).astype(BF16).astype(F32) + bias[...]
    fade = jnp.exp(-rate[...] * (jnp.maximum(xa, 0.0) + jnp.log1p(jnp.exp(-jnp.abs(xa)))))
    beta = jax.nn.sigmoid(nt_dot(normed, wb[...]).astype(BF16).astype(F32))
    for h in range(heads):
        fades[:, h, :] = jnp.broadcast_to(fade[:, h : h + 1], (seqs, dim))
        betas[:, h, :] = jnp.broadcast_to(beta[:, h : h + 1], (seqs, dim))
    w_copy(0).wait()
    raw_q = rounded(wbuf[0])
    w_copy(1).wait()
    raw_k = rounded(wbuf[1])
    for h in range(heads):
        cols = slice(h * dim, (h + 1) * dim)
        query = unit_rows(silu(raw_q[:, cols])) * dim ** (-0.5)
        key = unit_rows(silu(raw_k[:, cols]))
        kq[:, h, :] = key
        kq[:, heads + h, :] = query
        dots[:, h, :] = jnp.broadcast_to(jnp.sum(key * query, axis=-1, keepdims=True), (seqs, dim))
    w_copy(2).wait()
    value = silu(rounded(wbuf[2]))
    for h in range(heads):
        vals[:, h, :] = value[:, h * dim : (h + 1) * dim]
    w_copy(3).wait()
    zbuf[...] = silu(rounded(wbuf[3]))

    def one_chunk(c, carry):
        in_copy(c).wait()
        for i in range(step):
            s = c * step + i
            turned = kq[s].T
            fs, bs, vs, ds = fades[s], betas[s], vals[s], dots[s]
            for h in range(heads):
                block = st[s, h]
                kc = jnp.broadcast_to(turned[:, h : h + 1], (dim, dim))
                qc = jnp.broadcast_to(turned[:, heads + h : heads + h + 1], (dim, dim))
                f = fs[h : h + 1]
                pred = jnp.sum(block * kc, axis=0, keepdims=True)
                proj = jnp.sum(block * qc, axis=0, keepdims=True)
                written = bs[h : h + 1] * (vs[h : h + 1] - f * pred)
                ns[s, h] = f * block + kc * written
                reads[s, pl.ds(h, 1)] = f * proj + written * ds[h : h + 1]
        out_copy(c).start()
        return carry

    lax.fori_loop(0, chunks, one_chunk, 0)
    for h in range(heads):
        cols = slice(h * dim, (h + 1) * dim)
        heads_out[:, cols] = (rms_scale(reads[:, h, :], out_gain[...]) * zbuf[:, cols]).astype(BF16)
    for c in range(chunks):
        out_copy(c).wait()


def expert_kernel(
    n_ep,
    n_tp,
    top,
    cap,
    live,
    groups,
    tokens_ref,
    heads_out,
    w_out,
    gain_ref,
    w_gate,
    w_up,
    w_down,
    routes_ref,
    weights_ref,
    out,
    tokens,
    ffn_gain,
    routes,
    weights,
    wo,
    wg,
    wu,
    wdn,
    part_out,
    part_in,
    resid,
    moe,
    disp,
    arrived,
    acc_g,
    acc_u,
    other,
    other_in,
    mine,
    ret_out,
    ret_in,
    w_sem,
    part_sem,
    go_send,
    go_recv,
    fw_send,
    fw_recv,
    half_send,
    half_recv,
    back_send,
    back_recv,
):
    seqs, width = tokens.shape
    cols = width // n_tp
    e = lax.axis_index("ep")
    t = lax.axis_index("tp")
    u = n_tp - 1 - t
    used = pl.ds(0, live)

    def peer(i):
        return lax.rem(e + i, n_ep)

    def source(i):
        return lax.rem(e + n_ep - i, n_ep)

    partner = {"ep": e, "tp": u}
    mesh_ids = pl.DeviceIdType.MESH
    barrier = pltpu.get_barrier_semaphore()
    pl.semaphore_signal(barrier, inc=1, device_id=partner, device_id_type=mesh_ids)

    def greet(i, carry):
        pl.semaphore_signal(barrier, inc=1, device_id={"ep": peer(i), "tp": t}, device_id_type=mesh_ids)
        return carry

    lax.fori_loop(1, n_ep, greet, 0)

    loads = [
        pltpu.make_async_copy(src, dst, w_sem.at[n])
        for n, (src, dst) in enumerate(
            (
                (w_out, wo),
                (tokens_ref, tokens),
                (routes_ref, routes),
                (weights_ref, weights),
                (gain_ref, ffn_gain),
                (w_gate.at[0], wg),
                (w_up.at[0], wu),
                (w_down.at[0], wdn),
            )
        )
    ]
    for load in loads:
        load.start()
    for n in (1, 2, 3, 4):
        loads[n].wait()
    eye = lax.broadcasted_iota(jnp.int32, (seqs, seqs), 1) == lax.broadcasted_iota(
        jnp.int32, (seqs, seqs), 0
    )

    def column(row):
        return jnp.sum(jnp.where(eye, row, 0.0), axis=1, keepdims=True)

    lower = (
        lax.broadcasted_iota(jnp.int32, (seqs, seqs), 1)
        < lax.broadcasted_iota(jnp.int32, (seqs, seqs), 0)
    ).astype(BF16)
    picks = []
    taken = jnp.zeros((1, n_ep), F32)
    for j in range(top):
        route = column(routes[j : j + 1, :].astype(F32)).astype(jnp.int32)
        hot = lax.broadcasted_iota(jnp.int32, (seqs, n_ep), 1) == route
        hot_f = hot.astype(F32)
        before = jnp.dot(lower, hot_f.astype(BF16), preferred_element_type=F32) + taken
        slot = jnp.sum(before * hot_f, axis=1, keepdims=True).astype(jnp.int32)
        taken = taken + jnp.sum(hot_f, axis=0, keepdims=True)
        place = route * cap + slot
        picks.append(
            (lax.broadcasted_iota(jnp.int32, (seqs, n_ep * cap), 1) == place).astype(F32)
        )
    spread = sum(picks[1:], picks[0]).T.astype(BF16)

    loads[0].wait()
    part_out[...] = jnp.dot(heads_out[...], wo[...], preferred_element_type=F32).astype(BF16)
    pl.semaphore_wait(barrier, n_ep)

    swap = pltpu.make_async_remote_copy(
        src_ref=part_out,
        dst_ref=part_in,
        send_sem=part_sem.at[0],
        recv_sem=part_sem.at[1],
        device_id=partner,
        device_id_type=mesh_ids,
    )
    swap.start()
    swap.wait()
    rows = tokens[...].astype(F32) + (part_out[...].astype(F32) + part_in[...].astype(F32))
    resid[...] = rows
    moe[...] = rms_scale(rows, ffn_gain[...]).astype(BF16)
    own = pl.ds(pl.multiple_of(t * cols, 128), cols)
    far = pl.ds(pl.multiple_of(u * cols, 128), cols)
    going = jnp.dot(spread, moe[:, own], preferred_element_type=F32)
    disp[...] = going.reshape(n_ep, cap, cols).astype(BF16)

    def go(i):
        return pltpu.make_async_remote_copy(
            src_ref=disp.at[peer(i), used],
            dst_ref=arrived.at[t, e, used],
            send_sem=go_send.at[i],
            recv_sem=go_recv.at[i],
            device_id={"ep": peer(i), "tp": t},
            device_id_type=mesh_ids,
        )

    def forward(i):
        s = source(i)
        return pltpu.make_async_remote_copy(
            src_ref=arrived.at[t, s, used],
            dst_ref=arrived.at[t, s, used],
            send_sem=fw_send.at[i],
            recv_sem=fw_recv.at[i],
            device_id=partner,
            device_id_type=mesh_ids,
        )

    def go_start(i, carry):
        go(i).start()
        return carry

    lax.fori_loop(1, n_ep, go_start, 0)
    arrived[t, e] = disp[e]
    forward(0).start()

    def pass_on(i, carry):
        go(i).wait_recv()
        forward(i).start()
        return carry

    lax.fori_loop(1, n_ep, pass_on, 0)
    loads[5].wait()
    loads[6].wait()

    def half(which):
        got = arrived[which].astype(F32).reshape(n_ep * cap, cols).astype(BF16)
        part = pl.ds(pl.multiple_of(which * cols, 128), cols)
        return (
            jnp.dot(got, wg[part, :], preferred_element_type=F32),
            jnp.dot(got, wu[part, :], preferred_element_type=F32),
        )

    acc_g[...], acc_u[...] = half(t)

    def fw_done(i, carry):
        forward(i).wait_recv()
        return carry

    lax.fori_loop(0, n_ep, fw_done, 0)
    more_g, more_u = half(u)
    hidden = (silu(acc_g[...] + more_g) * (acc_u[...] + more_u)).astype(BF16)
    loads[7].wait()

    size = n_ep // groups

    def give(g):
        span = pl.ds(g * size, size)
        return pltpu.make_async_remote_copy(
            src_ref=other.at[span],
            dst_ref=other_in.at[span],
            send_sem=half_send.at[g],
            recv_sem=half_recv.at[g],
            device_id=partner,
            device_id_type=mesh_ids,
        )

    def back(s):
        i = lax.rem(e + n_ep - s, n_ep)
        return pltpu.make_async_remote_copy(
            src_ref=ret_out.at[s, used],
            dst_ref=ret_in.at[e, used],
            send_sem=back_send.at[i],
            recv_sem=back_recv.at[i],
            device_id={"ep": s, "tp": t},
            device_id_type=mesh_ids,
        )

    for g in range(groups):
        rows_g = hidden[g * size * cap : (g + 1) * size * cap]
        term = jnp.dot(rows_g, wdn[:, far], preferred_element_type=F32)
        other[pl.ds(g * size, size)] = term.reshape(size, cap, cols).astype(BF16)
        give(g).start()
    term = jnp.dot(hidden, wdn[:, own], preferred_element_type=F32)
    mine[...] = term.reshape(n_ep, cap, cols).astype(BF16)
    for g in range(groups):
        span = pl.ds(g * size, size)
        give(g).wait_recv()
        both = mine[span].astype(F32) + other_in[span].astype(F32)
        ret_out[span] = both.astype(BF16)

        def back_start(s, carry):
            @pl.when(s != e)
            def _():
                back(s).start()

            return carry

        lax.fori_loop(g * size, (g + 1) * size, back_start, 0)
    ret_in[e] = ret_out[e]

    def back_done(i, carry):
        back(source(i)).wait_recv()
        return carry

    lax.fori_loop(1, n_ep, back_done, 0)
    kept = lax.broadcasted_iota(jnp.int32, (n_ep, cap, cols), 1) < live
    returned = jnp.where(kept, ret_in[...].astype(F32), 0.0)
    returned = returned.reshape(n_ep * cap, cols).astype(BF16)
    total = resid[:, own]
    combined = None
    for j in range(top):
        found = jnp.dot(picks[j].astype(BF16), returned, preferred_element_type=F32)
        term = found * column(weights[j : j + 1, :])
        combined = term if combined is None else combined + term
    out[...] = (total + combined).astype(BF16)

    forward(0).wait_send()

    def sent(i, carry):
        go(i).wait_send()
        forward(i).wait_send()
        back(source(i)).wait_send()
        return carry

    lax.fori_loop(1, n_ep, sent, 0)
    for g in range(groups):
        give(g).wait_send()


def per_device(
    n_ep,
    n_tp,
    tokens,
    attn_gain,
    w_query,
    w_key,
    w_value,
    w_zgate,
    w_decay,
    w_beta,
    decay_rate,
    decay_bias,
    state,
    out_gain,
    w_out,
    ffn_gain,
    expert_gate,
    expert_up,
    expert_down,
    routes,
    route_weight,
):
    seqs, width = tokens.shape
    heads, dim = state.shape[1], state.shape[2]
    top = routes.shape[1]
    inner = heads * dim
    step = 2 if seqs % 2 == 0 else 1
    chunks = seqs // step
    heads_out, new_state = pl.pallas_call(
        functools.partial(mixer_kernel, step),
        out_shape=(
            pltpu.VMEM((seqs, inner), BF16),
            jax.ShapeDtypeStruct(state.shape, F32),
        ),
        in_specs=[HBM] * 12,
        out_specs=(VMEM, HBM),
        scratch_shapes=[
            pltpu.VMEM((seqs, width), BF16),
            pltpu.VMEM((1, width), F32),
            pltpu.VMEM((heads, width), BF16),
            pltpu.VMEM((heads, width), BF16),
            pltpu.VMEM((1, heads), F32),
            pltpu.VMEM((1, heads), F32),
            pltpu.VMEM((1, dim), F32),
            pltpu.SemaphoreType.DMA((7,)),
            pltpu.VMEM((4, width, inner), BF16),
            pltpu.VMEM(state.shape, F32),
            pltpu.VMEM(state.shape, F32),
            pltpu.VMEM((seqs, 2 * heads, dim), F32),
            pltpu.VMEM((seqs, heads, dim), F32),
            pltpu.VMEM((seqs, inner), F32),
            pltpu.VMEM((seqs, heads, dim), F32),
            pltpu.VMEM((seqs, heads, dim), F32),
            pltpu.VMEM((seqs, heads, dim), F32),
            pltpu.VMEM((seqs, heads, dim), F32),
            pltpu.SemaphoreType.DMA((4,)),
            pltpu.SemaphoreType.DMA((chunks,)),
            pltpu.SemaphoreType.DMA((chunks,)),
        ],
        compiler_params=pltpu.CompilerParams(vmem_limit_bytes=VMEM_LIMIT),
        name="mixer",
    )(
        tokens,
        attn_gain.reshape(1, width),
        w_query,
        w_key,
        w_value,
        w_zgate,
        w_decay.T,
        w_beta.T,
        decay_rate.reshape(1, heads),
        decay_bias.reshape(1, heads),
        state,
        out_gain.reshape(1, dim),
    )

    live = max(2, 2 * seqs * top // n_ep)
    cap = -(-live // 8) * 8
    cols = width // n_tp
    ff = expert_gate.shape[2]
    groups = 4 if n_ep % 4 == 0 else 1
    slots = (n_ep, cap, cols)
    dma = pltpu.SemaphoreType.DMA
    layer_out = pl.pallas_call(
        functools.partial(expert_kernel, n_ep, n_tp, top, cap, live, groups),
        out_shape=pltpu.VMEM((seqs, cols), BF16),
        in_specs=[HBM, VMEM] + [HBM] * 7,
        out_specs=VMEM,
        scratch_shapes=[
            pltpu.VMEM((seqs, width), BF16),
            pltpu.VMEM((1, width), F32),
            pltpu.VMEM((top, seqs), jnp.int32),
            pltpu.VMEM((top, seqs), F32),
            pltpu.VMEM((inner, width), BF16),
            pltpu.VMEM((width, ff), BF16),
            pltpu.VMEM((width, ff), BF16),
            pltpu.VMEM((ff, width), BF16),
            pltpu.VMEM((seqs, width), BF16),
            pltpu.VMEM((seqs, width), BF16),
            pltpu.VMEM((seqs, width), F32),
            pltpu.VMEM((seqs, width), BF16),
            pltpu.VMEM(slots, BF16),
            pltpu.VMEM((n_tp,) + slots, BF16),
            pltpu.VMEM((n_ep * cap, ff), F32),
            pltpu.VMEM((n_ep * cap, ff), F32),
            pltpu.VMEM(slots, BF16),
            pltpu.VMEM(slots, BF16),
            pltpu.VMEM(slots, BF16),
            pltpu.VMEM(slots, BF16),
            pltpu.VMEM(slots, BF16),
            dma((8,)),
            dma((2,)),
            dma((n_ep,)),
            dma((n_ep,)),
            dma((n_ep,)),
            dma((n_ep,)),
            dma((groups,)),
            dma((groups,)),
            dma((n_ep,)),
            dma((n_ep,)),
        ],
        compiler_params=pltpu.CompilerParams(
            collective_id=0, has_side_effects=True, vmem_limit_bytes=VMEM_LIMIT - 2**21
        ),
        name="experts",
    )(
        tokens,
        pltpu.with_memory_space_constraint(heads_out, pltpu.VMEM),
        w_out,
        ffn_gain.reshape(1, width),
        expert_gate,
        expert_up,
        expert_down,
        routes.T,
        route_weight.T,
    )
    return (layer_out, new_state)


def solution(mesh):
    in_specs = (
        P("ep", None),
        P(),
        P(None, "tp"),
        P(None, "tp"),
        P(None, "tp"),
        P(None, "tp"),
        P(None, "tp"),
        P(None, "tp"),
        P("tp"),
        P("tp"),
        P("ep", "tp", None, None),
        P(),
        P("tp", None),
        P(),
        P("ep", None, "tp"),
        P("ep", None, "tp"),
        P("ep", "tp", None),
        P("ep", None),
        P("ep", None),
    )
    out_specs = (P("ep", "tp"), P("ep", "tp", None, None))
    body = functools.partial(per_device, mesh.shape["ep"], mesh.shape["tp"])
    return jax.shard_map(body, mesh=mesh, in_specs=in_specs, out_specs=out_specs, check_vma=False)
```

profile of v0, /device:TPU:0, one launch (start us, length us, event | category | flops | bytes accessed | tf_op | source)
XLA Modules:
  0.0 39.2 jit_solution(16311722495002985502)
XLA Ops:
  0.6 13.5 %mixer.1 = (bf16[24,512]{1,0:T(8,128)(2,1)S(1)}, f32[24,4,128,128]{3,2,1,0:T(8,128)}) custom-call(bf16[24,2048]{1,0:T(8,128)(2,1)} %tokens_ref.3, f32[1,2048]{1,0:T(1,128)} %bitcast.11, bf16[2048,512]{1,0:T(8,128)(2,1)} %wq.1, bf16[2048,512]{1,0:T(8,128)(2,1)} %wk.1, bf16[2048,512]{1,0:T(8,128)(2,1)} %wv.1, bf16[2048,512]{1,0:T(8,128)(2,1)} %wz.1, ...), custom_call_target="tpu_custom_call" | custom-call | tf_op jit(solution)/shard_map/mixer/pallas_call | solution.py:467
  14.1 24.4 %experts.1 = bf16[24,1024]{1,0:T(8,128)(2,1)S(1)} custom-call(bf16[24,2048]{1,0:T(8,128)(2,1)} %tokens_ref.3, bf16[24,512]{1,0:T(8,128)(2,1)S(1)} %get-tuple-element.4.heads_out, bf16[512,2048]{1,0:T(8,128)(2,1)} %w_out.1, f32[1,2048]{1,0:T(1,128)} %bitcast.12, bf16[1,2048,256]{2,1,0:T(8,128)(2,1)} %w_gate.1, bf16[1,2048,256]{2,1,0:T(8,128)(2,1)} %w_up.1, ...), custom_call_target="tpu_custom_call" | custom-call | tf_op jit(solution)/shard_map/experts/pallas_call | solution.py:522
  38.6 0.6 %copy.22 = bf16[24,1024]{1,0:T(8,128)(2,1)} copy(bf16[24,1024]{1,0:T(8,128)(2,1)S(1)} %experts.1) | data formatting | bytes 98304
where the time goes:
time: 39.3 us; the launch traced here: 39.2 us
  Pallas kernels  37.9 us (96%)
  between operations  0.65 us (2%)
  local copies, waits for them, and re-layouts  0.62 us (2%)
    pallas_call x1, Pallas kernels, per_device(): pl.pallas_call(functools.partial(expert_kernel, n_ep, n_tp, top, cap, liv...  24.4 us
    pallas_call x1, Pallas kernels, per_device(): pl.pallas_call(functools.partial(mixer_kernel, step), out_shape=(pltpu.VM...  13.5 us

commit v1 on v0

v1 whole, which is shorter than its diff:
```python
import functools

import jax
import jax.numpy as jnp
from jax import lax
from jax.experimental import pallas as pl
from jax.experimental.pallas import tpu as pltpu
from jax.sharding import PartitionSpec as P

EPS = 1e-06
F32 = jnp.float32
BF16 = jnp.bfloat16
VMEM_LIMIT = 44 * 1024 * 1024
HBM = pl.BlockSpec(memory_space=pltpu.HBM)
VMEM = pl.BlockSpec(memory_space=pltpu.VMEM)


def rms_scale(rows, gain):
    return rows * lax.rsqrt(jnp.mean(rows * rows, axis=-1, keepdims=True) + EPS) * gain


def unit_rows(rows):
    return rows * lax.rsqrt(jnp.sum(rows * rows, axis=-1, keepdims=True) + EPS)


def silu(x):
    return x * jax.nn.sigmoid(x)


def nt_dot(rows, weight):
    return lax.dot_general(rows, weight, (((1,), (1,)), ((), ())), preferred_element_type=F32)


def iota(shape, axis):
    return lax.broadcasted_iota(jnp.int32, shape, axis)


def layer_kernel(
    n_ep,
    n_tp,
    top,
    cap,
    shares,
    step,
    tokens_ref,
    attn_ref,
    wd_ref,
    wb_ref,
    rate_ref,
    bias_ref,
    og_ref,
    ffn_ref,
    routes_ref,
    weights_ref,
    wq,
    wk,
    wv,
    wz,
    state,
    w_out,
    w_gate,
    w_up,
    w_down,
    out,
    ns,
    tokens,
    attn_gain,
    wd,
    wb,
    rate,
    bias,
    out_gain,
    ffn_gain,
    routes,
    weights,
    wbuf,
    wo,
    wg,
    wu,
    wdn,
    kq,
    vals,
    zbuf,
    fades,
    betas,
    dots,
    reads,
    spread,
    picks,
    part_out,
    part_in,
    resid,
    disp,
    arrived,
    ret_out,
    ret_in,
    small_sem,
    w_sem,
    in_sem,
    x_sem,
    part_sem,
    push_sem,
    go_sem,
    back_sem,
    back_recv,
):
    seqs, heads, dim, _ = ns.shape
    width = tokens.shape[1]
    cols = width // n_tp
    chunks = seqs // step
    e = lax.axis_index("ep")
    t = lax.axis_index("tp")
    u = n_tp - 1 - t
    mesh_ids = pl.DeviceIdType.MESH
    partner = {"ep": e, "tp": u}
    barrier = pltpu.get_barrier_semaphore()
    pl.semaphore_signal(barrier, inc=1, device_id=partner, device_id_type=mesh_ids)

    def far(i):
        k = (i + 1) // 2
        return lax.rem(e + n_ep // 2 + k * (2 * lax.rem(i, 2) - 1) + n_ep, n_ep)

    def greet(i, carry):
        pl.semaphore_signal(barrier, inc=1, device_id={"ep": far(i), "tp": t}, device_id_type=mesh_ids)
        return carry

    lax.fori_loop(0, n_ep - 1, greet, 0)

    def in_copy(c):
        rows = pl.ds(c * step, step)
        return pltpu.make_async_copy(state.at[rows], ns.at[rows], in_sem.at[c])

    small = [
        pltpu.make_async_copy(src, dst, small_sem.at[n])
        for n, (src, dst) in enumerate(
            (
                (tokens_ref, tokens),
                (attn_ref, attn_gain),
                (wd_ref, wd),
                (wb_ref, wb),
                (rate_ref, rate),
                (bias_ref, bias),
                (og_ref, out_gain),
                (ffn_ref, ffn_gain),
                (routes_ref, routes),
                (weights_ref, weights),
            )
        )
    ]
    load = [pltpu.make_async_copy(src, wbuf.at[n], w_sem.at[n]) for n, src in enumerate((wq, wk, wv, wz))]
    load.append(pltpu.make_async_copy(w_out, wo, w_sem.at[4]))
    experts = [
        pltpu.make_async_copy(src.at[0], dst.at[t], x_sem.at[n])
        for n, (src, dst) in enumerate(((w_gate, wg), (w_up, wu), (w_down, wdn)))
    ]
    push = [
        pltpu.make_async_remote_copy(
            src_ref=dst.at[t],
            dst_ref=dst.at[t],
            send_sem=push_sem.at[0, n],
            recv_sem=push_sem.at[1, n],
            device_id=partner,
            device_id_type=mesh_ids,
        )
        for n, dst in enumerate((wg, wu, wdn))
    ]
    for copy in small:
        copy.start()
    for n in range(3):
        load[n].start()
    for copy in small:
        copy.wait()
    lax.fori_loop(0, chunks, lambda c, carry: (in_copy(c).start(), carry)[1], 0)

    normed = rms_scale(tokens[...].astype(F32), attn_gain[...]).astype(BF16)

    def rounded(weight):
        return jnp.dot(normed, weight, preferred_element_type=F32).astype(BF16).astype(F32)

    xa = nt_dot(normed, wd[...]).astype(BF16).astype(F32) + bias[...]
    fade = jnp.exp(-rate[...] * (jnp.maximum(xa, 0.0) + jnp.log1p(jnp.exp(-jnp.abs(xa)))))
    beta = jax.nn.sigmoid(nt_dot(normed, wb[...]).astype(BF16).astype(F32))
    for h in range(heads):
        fades[:, h, :] = jnp.broadcast_to(fade[:, h : h + 1], (seqs, dim))
        betas[:, h, :] = jnp.broadcast_to(beta[:, h : h + 1], (seqs, dim))

    eye = iota((seqs, seqs), 1) == iota((seqs, seqs), 0)

    def column(row):
        return jnp.sum(jnp.where(eye, row, 0.0), axis=1, keepdims=True)

    lower = (iota((seqs, seqs), 1) < iota((seqs, seqs), 0)).astype(BF16)
    slots = n_ep * cap
    taken = jnp.zeros((1, n_ep), F32)
    found = []
    mine = jnp.zeros((seqs, slots), F32)
    for j in range(top):
        route = column(routes[j : j + 1, :].astype(F32)).astype(jnp.int32)
        hot = (iota((seqs, n_ep), 1) == route).astype(F32)
        before = jnp.dot(lower, hot.astype(BF16), preferred_element_type=F32) + taken
        slot = jnp.sum(before * hot, axis=1, keepdims=True).astype(jnp.int32)
        taken = taken + jnp.sum(hot, axis=0, keepdims=True)
        place = route * cap + slot + jnp.where(slot < shares[0], 0, slots - shares[0])
        found.append((iota((seqs, n_tp * slots), 1) == place).astype(F32))
        mine = mine + (iota((seqs, slots), 1) + t * slots == place).astype(F32)
    spread[...] = mine.T.astype(BF16)
    picks[...] = jnp.concatenate(found, axis=0).astype(BF16)

    load[0].wait()
    raw_q = rounded(wbuf[0])
    load[1].wait()
    raw_k = rounded(wbuf[1])
    for n in (3, 4):
        load[n].start()
    for h in range(heads):
        span = slice(h * dim, (h + 1) * dim)
        query = unit_rows(silu(raw_q[:, span])) * dim ** (-0.5)
        key = unit_rows(silu(raw_k[:, span]))
        kq[:, h, :] = key
        kq[:, heads + h, :] = query
        dots[:, h, :] = jnp.broadcast_to(jnp.sum(key * query, axis=-1, keepdims=True), (seqs, dim))
    load[2].wait()
    value = silu(rounded(wbuf[2]))
    for h in range(heads):
        vals[:, h, :] = value[:, h * dim : (h + 1) * dim]
    for copy in experts:
        copy.start()

    def one_chunk(c, carry):
        in_copy(c).wait()
        hits = []
        for i in range(step):
            s = c * step + i
            lhs = kq[s].astype(BF16)
            hits.append([jnp.dot(lhs, ns[s, h].astype(BF16), preferred_element_type=F32) for h in range(heads)])
        for i in range(step):
            s = c * step + i
            turned = kq[s].T
            fs, bs, vs, ds = fades[s], betas[s], vals[s], dots[s]
            for h in range(heads):
                hit = hits[i][h]
                f = fs[h : h + 1]
                written = bs[h : h + 1] * (vs[h : h + 1] - f * hit[h : h + 1])
                kc = jnp.broadcast_to(turned[:, h : h + 1], (dim, dim))
                ns[s, h] = f * ns[s, h] + kc * written
                reads[s, pl.ds(h, 1)] = f * hit[heads + h : heads + h + 1] + written * ds[h : h + 1]
        return carry

    lax.fori_loop(0, chunks, one_chunk, 0)
    load[3].wait()
    zbuf[...] = silu(rounded(wbuf[3]))
    mixed = []
    for h in range(heads):
        span = slice(h * dim, (h + 1) * dim)
        mixed.append((rms_scale(reads[:, h, :], out_gain[...]) * zbuf[:, span]).astype(BF16))
    load[4].wait()
    part_out[...] = jnp.dot(jnp.concatenate(mixed, axis=1), wo[...], preferred_element_type=F32).astype(BF16)
    pl.semaphore_wait(barrier, n_ep)

    swap = pltpu.make_async_remote_copy(
        src_ref=part_out,
        dst_ref=part_in,
        send_sem=part_sem.at[0],
        recv_sem=part_sem.at[1],
        device_id=partner,
        device_id_type=mesh_ids,
    )
    swap.start()
    experts[0].wait()
    push[0].start()
    swap.wait()
    rows = tokens[...].astype(F32) + (part_out[...].astype(F32) + part_in[...].astype(F32))
    resid[...] = rows
    moe = rms_scale(rows, ffn_gain[...]).astype(BF16)
    going = jnp.dot(spread[...], moe, preferred_element_type=F32)
    disp[...] = going.reshape(n_ep, cap, width).astype(BF16)

    def go(n, p):
        return pltpu.make_async_remote_copy(
            src_ref=disp.at[p, pl.ds(0, n)],
            dst_ref=arrived.at[e, pl.ds(0, n)],
            send_sem=go_sem.at[0],
            recv_sem=go_sem.at[1],
            device_id={"ep": p, "tp": t},
            device_id_type=mesh_ids,
        )

    def all_go(n, which):
        block = arrived.at[pl.ds(0, n_ep - 1), pl.ds(0, n)]
        return pltpu.make_async_copy(block, block, go_sem.at[which])

    def back(n, c, p):
        return pltpu.make_async_remote_copy(
            src_ref=ret_out.at[c, p, pl.ds(0, n)],
            dst_ref=ret_in.at[t, e, pl.ds(0, n)],
            send_sem=back_sem.at[0],
            recv_sem=back_recv.at[t],
            device_id={"ep": p, "tp": c},
            device_id_type=mesh_ids,
        )

    def all_back(n, c, count, sem):
        block = ret_in.at[c, pl.ds(0, count), pl.ds(0, n)]
        return pltpu.make_async_copy(block, block, sem)

    for c, n in enumerate(shares):
        if n:

            @pl.when(t == c)
            def _(n=n):
                lax.fori_loop(0, n_ep - 1, lambda i, carry: (go(n, far(i)).start(), carry)[1], 0)

    arrived[e] = disp[e]
    for n in (1, 2):
        experts[n].wait()
        push[n].start()
    for c, n in enumerate(shares):
        if n:

            @pl.when(t == c)
            def _(n=n):
                all_go(n, 1).wait()

    got = arrived[...].astype(F32).reshape(slots, width).astype(BF16)
    push[0].wait_recv()
    gates = [jnp.dot(got, wg[h], preferred_element_type=F32) for h in range(n_tp)]
    push[1].wait_recv()
    ups = [jnp.dot(got, wu[h], preferred_element_type=F32) for h in range(n_tp)]
    hidden = [(silu(gates[h]) * ups[h]).astype(BF16) for h in range(n_tp)]
    push[2].wait_recv()
    for c in range(n_tp):
        term = None
        for h in range(n_tp):
            piece = jnp.dot(hidden[h], wdn[h, :, c * cols : (c + 1) * cols], preferred_element_type=F32)
            term = piece if term is None else term + piece
        ret_out[c] = term.reshape(n_ep, cap, cols).astype(BF16)

    for c, n in enumerate(shares):
        if n:

            @pl.when(t == c)
            def _(n=n, c=c):
                def send(i, carry):
                    for d in range(n_tp):
                        back(n, d, far(i)).start()
                    return carry

                lax.fori_loop(0, n_ep - 1, send, 0)
                for d in range(n_tp):
                    if d != c:
                        back(n, d, e).start()

    ret_in[t, e] = ret_out[t, e]
    total = resid[:, pl.ds(pl.multiple_of(t * cols, 128), cols)]
    scale = [column(weights[j : j + 1, :]) for j in range(top)]
    for c, n in enumerate(shares):
        if n:
            for d in range(n_tp):

                @pl.when(t == d)
                def _(n=n, c=c, d=d):
                    all_back(n, c, n_ep - (c == d), back_recv.at[c]).wait()

    kept = [(iota((n_ep, cap, cols), 1) < n) for n in shares]
    returned = [
        jnp.where(kept[c], ret_in[c].astype(F32), 0.0).reshape(slots, cols).astype(BF16) for c in range(n_tp)
    ]
    combined = jnp.dot(picks[...], jnp.concatenate(returned, axis=0), preferred_element_type=F32)
    for j in range(top):
        total = total + combined[j * seqs : (j + 1) * seqs] * scale[j]
    out[...] = total.astype(BF16)

    for copy in push:
        copy.wait_send()
    for c, n in enumerate(shares):
        if n:

            @pl.when(t == c)
            def _(n=n):
                all_go(n, 0).wait()
                for d in range(n_tp):
                    all_back(n, d, n_ep - 1 + d, back_sem.at[0]).wait()


def per_device(
    n_ep,
    n_tp,
    tokens,
    attn_gain,
    w_query,
    w_key,
    w_value,
    w_zgate,
    w_decay,
    w_beta,
    decay_rate,
    decay_bias,
    state,
    out_gain,
    w_out,
    ffn_gain,
    expert_gate,
    expert_up,
    expert_down,
    routes,
    route_weight,
):
    seqs, width = tokens.shape
    heads, dim = state.shape[1], state.shape[2]
    top = routes.shape[1]
    inner = heads * dim
    step = 4 if seqs % 4 == 0 else 1
    chunks = seqs // step
    live = max(2, 2 * seqs * top // n_ep)
    first = 2 * -(-live // 4)
    shares = (first, live - first)
    cap = -(-first // 8) * 8
    cols = width // n_tp
    ff = expert_gate.shape[2]
    slots = n_ep * cap
    vmem = pltpu.VMEM
    dma = pltpu.SemaphoreType.DMA
    return pl.pallas_call(
        functools.partial(layer_kernel, n_ep, n_tp, top, cap, shares, step),
        out_shape=(vmem((seqs, cols), BF16), vmem(state.shape, F32)),
        in_specs=[HBM] * 19,
        out_specs=(VMEM, VMEM),
        scratch_shapes=[
            vmem((seqs, width), BF16),
            vmem((1, width), F32),
            vmem((heads, width), BF16),
            vmem((heads, width), BF16),
            vmem((1, heads), F32),
            vmem((1, heads), F32),
            vmem((1, dim), F32),
            vmem((1, width), F32),
            vmem((top, seqs), jnp.int32),
            vmem((top, seqs), F32),
            vmem((4, width, inner), BF16),
            vmem((inner, width), BF16),
            vmem((n_tp, width, ff), BF16),
            vmem((n_tp, width, ff), BF16),
            vmem((n_tp, ff, width), BF16),
            vmem((seqs, 2 * heads, dim), F32),
            vmem((seqs, heads, dim), F32),
            vmem((seqs, inner), F32),
            vmem((seqs, heads, dim), F32),
            vmem((seqs, heads, dim), F32),
            vmem((seqs, heads, dim), F32),
            vmem((seqs, heads, dim), F32),
            vmem((slots, seqs), BF16),
            vmem((top * seqs, n_tp * slots), BF16),
            vmem((seqs, width), BF16),
            vmem((seqs, width), BF16),
            vmem((seqs, width), F32),
            vmem((n_ep, cap, width), BF16),
            vmem((n_ep, cap, width), BF16),
            vmem((n_tp, n_ep, cap, cols), BF16),
            vmem((n_tp, n_ep, cap, cols), BF16),
            dma((10,)),
            dma((5,)),
            dma((chunks,)),
            dma((3,)),
            dma((2,)),
            dma((2, 3)),
            dma((2,)),
            dma((1,)),
            dma((n_tp,)),
        ],
        compiler_params=pltpu.CompilerParams(
            collective_id=0, has_side_effects=True, vmem_limit_bytes=VMEM_LIMIT
        ),
        name="layer",
    )(
        tokens,
        attn_gain.reshape(1, width),
        w_decay.T,
        w_beta.T,
        decay_rate.reshape(1, heads),
        decay_bias.reshape(1, heads),
        out_gain.reshape(1, dim),
        ffn_gain.reshape(1, width),
        routes.T,
        route_weight.T,
        w_query,
        w_key,
        w_value,
        w_zgate,
        state,
        w_out,
        expert_gate,
        expert_up,
        expert_down,
    )


def solution(mesh):
    in_specs = (
        P("ep", None),
        P(),
        P(None, "tp"),
        P(None, "tp"),
        P(None, "tp"),
        P(None, "tp"),
        P(None, "tp"),
        P(None, "tp"),
        P("tp"),
        P("tp"),
        P("ep", "tp", None, None),
        P(),
        P("tp", None),
        P(),
        P("ep", None, "tp"),
        P("ep", None, "tp"),
        P("ep", "tp", None),
        P("ep", None),
        P("ep", None),
    )
    out_specs = (P("ep", "tp"), P("ep", "tp", None, None))
    body = functools.partial(per_device, mesh.shape["ep"], mesh.shape["tp"])
    return jax.shard_map(body, mesh=mesh, in_specs=in_specs, out_specs=out_specs, check_vma=False)
```

time: 39.3 us -> 42.6 us (1.084); the launches traced: 39.2 us -> 42.1 us
  local copies, waits for them, and re-layouts: 0.62 us -> 14 us
  Pallas kernels: 37.9 us -> 27.4 us
    unnamed x1 -> x28, local copies, waits for them, and re-layouts: 0.62 us -> 14 us
    pallas_call x2 -> x1, Pallas kernels: 37.9 us -> 27.4 us  [per_device(): pl.pallas_call(functools.partial(layer_kernel, n_ep, n_tp, top, cap, shar...]
where the time goes in v1:
time: 42.6 us; the launch traced here: 42.1 us
  Pallas kernels  27.4 us (64%)
  local copies, waits for them, and re-layouts  14 us (33%)
  between operations  0.67 us (2%)
    pallas_call x1, Pallas kernels, per_device(): pl.pallas_call(functools.partial(layer_kernel, n_ep, n_tp, top, cap, shar...  27.4 us
    unnamed x28, local copies, waits for them, and re-layouts  14 us

profile of v1, /device:TPU:0, one launch (start us, length us, event | category | flops | bytes accessed | tf_op | source)
XLA Modules:
  0.0 42.1 jit_solution(3509902702058712103)
XLA Ops:
  0.6 0.0 copy-start
  0.6 1.2 %copy-done = bf16[1,2048,256]{2,1,0:T(8,128)(2,1)S(1)} copy-done((bf16[1,2048,256]{2,1,0:T(8,128)(2,1)S(1)}, bf16[1,2048,256]{2,1,0:T(8,128)(2,1)}, u32[]{:S(2)}) %copy-start) | copy-done | bytes 1048600
  1.9 0.0 copy-start.1
  1.9 1.2 %copy-done.1 = bf16[1,2048,256]{2,1,0:T(8,128)(2,1)S(1)} copy-done((bf16[1,2048,256]{2,1,0:T(8,128)(2,1)S(1)}, bf16[1,2048,256]{2,1,0:T(8,128)(2,1)}, u32[]{:S(2)}) %copy-start.1) | copy-done | bytes 1048600
  3.1 0.0 copy-start.2
  3.1 1.2 %copy-done.2 = bf16[1,256,2048]{2,1,0:T(8,128)(2,1)S(1)} copy-done((bf16[1,256,2048]{2,1,0:T(8,128)(2,1)S(1)}, bf16[1,256,2048]{2,1,0:T(8,128)(2,1)}, u32[]{:S(2)}) %copy-start.2) | copy-done | bytes 1048600
  4.3 0.0 copy-start.3
  4.3 0.9 %copy-done.3 = bf16[24,2048]{1,0:T(8,128)(2,1)S(1)} copy-done((bf16[24,2048]{1,0:T(8,128)(2,1)S(1)}, bf16[24,2048]{1,0:T(8,128)(2,1)}, u32[]{:S(2)}) %copy-start.3) | copy-done | bytes 98328
  5.2 0.0 copy-start.4
  5.2 0.7 %copy-done.4 = bf16[2048,4]{0,1:T(4,128)(2,1)S(1)} copy-done((bf16[2048,4]{0,1:T(4,128)(2,1)S(1)}, bf16[2048,4]{0,1:T(4,128)(2,1)}, u32[]{:S(2)}) %copy-start.4) | copy-done | bytes 16408
  5.9 0.0 copy-start.5
  5.9 0.7 %copy-done.5 = bf16[2048,4]{0,1:T(4,128)(2,1)S(1)} copy-done((bf16[2048,4]{0,1:T(4,128)(2,1)S(1)}, bf16[2048,4]{0,1:T(4,128)(2,1)}, u32[]{:S(2)}) %copy-start.5) | copy-done | bytes 16408
  6.6 0.0 copy-start.6
  6.6 0.7 %copy-done.6 = f32[2048]{0:T(1024)S(1)} copy-done((f32[2048]{0:T(1024)S(1)}, f32[2048]{0:T(1024)}, u32[]{:S(2)}) %copy-start.6) | copy-done | bytes 8216
  7.3 0.0 copy-start.7
  7.3 0.7 %copy-done.7 = f32[2048]{0:T(1024)S(1)} copy-done((f32[2048]{0:T(1024)S(1)}, f32[2048]{0:T(1024)}, u32[]{:S(2)}) %copy-start.7) | copy-done | bytes 8216
  8.0 0.0 copy-start.8
  8.0 0.7 %copy-done.8 = s32[24,2]{0,1:T(2,128)S(1)} copy-done((s32[24,2]{0,1:T(2,128)S(1)}, s32[24,2]{0,1:T(2,128)}, u32[]{:S(2)}) %copy-start.8) | copy-done | bytes 216
  8.7 0.0 copy-start.9
  8.7 0.7 %copy-done.9 = f32[24,2]{0,1:T(2,128)S(1)} copy-done((f32[24,2]{0,1:T(2,128)S(1)}, f32[24,2]{0,1:T(2,128)}, u32[]{:S(2)}) %copy-start.9) | copy-done | bytes 216
  9.4 0.0 copy-start.10
  9.4 0.7 %copy-done.10 = f32[4]{0:T(128)S(1)} copy-done((f32[4]{0:T(128)S(1)}, f32[4]{0:T(128)}, u32[]{:S(2)}) %copy-start.10) | copy-done | bytes 40
  10.1 0.0 copy-start.11
  10.1 0.7 %copy-done.11 = f32[4]{0:T(128)S(1)} copy-done((f32[4]{0:T(128)S(1)}, f32[4]{0:T(128)}, u32[]{:S(2)}) %copy-start.11) | copy-done | bytes 40
  10.7 0.0 copy-start.12
  10.7 0.7 %copy-done.12 = f32[128]{0:T(128)S(1)} copy-done((f32[128]{0:T(128)S(1)}, f32[128]{0:T(128)}, u32[]{:S(2)}) %copy-start.12) | copy-done | bytes 536
  11.4 27.4 %layer.1 = (bf16[24,1024]{1,0:T(8,128)(2,1)S(1)}, f32[24,4,128,128]{3,2,1,0:T(8,128)S(1)}) custom-call(bf16[24,2048]{1,0:T(8,128)(2,1)S(1)} %copy-done.3, f32[1,2048]{1,0:T(1,128)S(1)} %bitcast.11, bf16[4,2048]{1,0:T(4,128)(2,1)S(1)} %bitcast.9, bf16[4,2048]{1,0:T(4,128)(2,1)S(1)} %bitcast.10, f32[1,4]{1,0:T(1,128)S(1)} %bitcast.15, f32[1,4]{1,0:T(1,128)S(1)} %bitcast.16, ...), custom_call_target="tpu_custom_call" | custom-call | tf_op jit(solution)/shard_map/layer/pallas_call | solution.py:423
  38.7 0.6 %copy.23 = bf16[24,1024]{1,0:T(8,128)(2,1)} copy(bf16[24,1024]{1,0:T(8,128)(2,1)S(1)} %get-tuple-element.2) | data formatting | bytes 98304
  39.4 2.7 %copy.24 = f32[24,4,128,128]{3,2,1,0:T(8,128)} copy(f32[24,4,128,128]{3,2,1,0:T(8,128)S(1)} %get-tuple-element.3) | data formatting | bytes 12582912
Async XLA Ops:
  0.6 1.2 %copy-start = (bf16[1,2048,256]{2,1,0:T(8,128)(2,1)S(1)}, bf16[1,2048,256]{2,1,0:T(8,128)(2,1)}, u32[]{:S(2)}) copy-start(bf16[1,2048,256]{2,1,0:T(8,128)(2,1)} %w_gate.1) | copy-start | bytes 3145732
  1.9 1.2 %copy-start.1 = (bf16[1,2048,256]{2,1,0:T(8,128)(2,1)S(1)}, bf16[1,2048,256]{2,1,0:T(8,128)(2,1)}, u32[]{:S(2)}) copy-start(bf16[1,2048,256]{2,1,0:T(8,128)(2,1)} %w_up.1) | copy-start | bytes 3145732
  3.1 1.2 %copy-start.2 = (bf16[1,256,2048]{2,1,0:T(8,128)(2,1)S(1)}, bf16[1,256,2048]{2,1,0:T(8,128)(2,1)}, u32[]{:S(2)}) copy-start(bf16[1,256,2048]{2,1,0:T(8,128)(2,1)} %w_down.1) | copy-start | bytes 3145732
  4.3 0.9 %copy-start.3 = (bf16[24,2048]{1,0:T(8,128)(2,1)S(1)}, bf16[24,2048]{1,0:T(8,128)(2,1)}, u32[]{:S(2)}) copy-start(bf16[24,2048]{1,0:T(8,128)(2,1)} %tokens_ref.1) | copy-start | bytes 294916
  5.2 0.7 %copy-start.4 = (bf16[2048,4]{0,1:T(4,128)(2,1)S(1)}, bf16[2048,4]{0,1:T(4,128)(2,1)}, u32[]{:S(2)}) copy-start(bf16[2048,4]{0,1:T(4,128)(2,1)} %param.25) | copy-start | bytes 49156
  5.9 0.7 %copy-start.5 = (bf16[2048,4]{0,1:T(4,128)(2,1)S(1)}, bf16[2048,4]{0,1:T(4,128)(2,1)}, u32[]{:S(2)}) copy-start(bf16[2048,4]{0,1:T(4,128)(2,1)} %param.26) | copy-start | bytes 49156
  6.6 0.7 %copy-start.6 = (f32[2048]{0:T(1024)S(1)}, f32[2048]{0:T(1024)}, u32[]{:S(2)}) copy-start(f32[2048]{0:T(1024)} %param.20) | copy-start | bytes 24580
  7.3 0.7 %copy-start.7 = (f32[2048]{0:T(1024)S(1)}, f32[2048]{0:T(1024)}, u32[]{:S(2)}) copy-start(f32[2048]{0:T(1024)} %param.32) | copy-start | bytes 24580
  8.0 0.7 %copy-start.8 = (s32[24,2]{0,1:T(2,128)S(1)}, s32[24,2]{0,1:T(2,128)}, u32[]{:S(2)}) copy-start(s32[24,2]{0,1:T(2,128)} %param.36) | copy-start | bytes 580
  8.7 0.7 %copy-start.9 = (f32[24,2]{0,1:T(2,128)S(1)}, f32[24,2]{0,1:T(2,128)}, u32[]{:S(2)}) copy-start(f32[24,2]{0,1:T(2,128)} %param.37) | copy-start | bytes 580
  9.4 0.7 %copy-start.10 = (f32[4]{0:T(128)S(1)}, f32[4]{0:T(128)}, u32[]{:S(2)}) copy-start(f32[4]{0:T(128)} %param.27) | copy-start | bytes 52
  10.1 0.7 %copy-start.11 = (f32[4]{0:T(128)S(1)}, f32[4]{0:T(128)}, u32[]{:S(2)}) copy-start(f32[4]{0:T(128)} %param.28) | copy-start | bytes 52
  10.7 0.7 %copy-start.12 = (f32[128]{0:T(128)S(1)}, f32[128]{0:T(128)}, u32[]{:S(2)}) copy-start(f32[128]{0:T(128)} %param.30) | copy-start | bytes 1540

commit v2 on v1

--- a/solution.py
+++ b/solution.py
@@ -10,7 +10,7 @@
 EPS = 1e-06
 F32 = jnp.float32
 BF16 = jnp.bfloat16
-VMEM_LIMIT = 44 * 1024 * 1024
+VMEM_LIMIT = 57 * 1024 * 1024
 HBM = pl.BlockSpec(memory_space=pltpu.HBM)
 VMEM = pl.BlockSpec(memory_space=pltpu.VMEM)
 
@@ -84,6 +84,7 @@
     fades,
     betas,
     dots,
+    turned,
     reads,
     spread,
     picks,
@@ -116,12 +117,22 @@
     barrier = pltpu.get_barrier_semaphore()
     pl.semaphore_signal(barrier, inc=1, device_id=partner, device_id_type=mesh_ids)
 
-    def far(i):
-        k = (i + 1) // 2
-        return lax.rem(e + n_ep // 2 + k * (2 * lax.rem(i, 2) - 1) + n_ep, n_ep)
+    bits = [1 << b for b in range((n_ep - 1).bit_length())] if n_ep & (n_ep - 1) == 0 else []
+    flips = [bit * (1 - 2 * lax.rem(e // bit, 2)) for bit in bits]
+
+    def across(i):
+        if not bits:
+            return lax.rem(e + 1 + i, n_ep)
+        p = e
+        for bit, flip in zip(bits, flips):
+            p = p + flip * lax.rem((n_ep - 1 - i) // bit, 2)
+        return p
+
+    def rising(i):
+        return lax.rem(i + jnp.where(i >= e, 1, 0), n_ep)
 
     def greet(i, carry):
-        pl.semaphore_signal(barrier, inc=1, device_id={"ep": far(i), "tp": t}, device_id_type=mesh_ids)
+        pl.semaphore_signal(barrier, inc=1, device_id={"ep": rising(i), "tp": t}, device_id_type=mesh_ids)
         return carry
 
     lax.fori_loop(0, n_ep - 1, greet, 0)
@@ -147,8 +158,14 @@
             )
         )
     ]
-    load = [pltpu.make_async_copy(src, wbuf.at[n], w_sem.at[n]) for n, src in enumerate((wq, wk, wv, wz))]
-    load.append(pltpu.make_async_copy(w_out, wo, w_sem.at[4]))
+    weight = [(src, wbuf.at[n]) for n, src in enumerate((wq, wk, wv, wz))] + [(w_out, wo)]
+
+    def load_start(n):
+        pltpu.make_async_copy(*weight[n], w_sem.at[n]).start()
+
+    def load_wait(n):
+        pltpu.make_async_copy(*weight[n], w_sem.at[n]).wait()
+
     experts = [
         pltpu.make_async_copy(src.at[0], dst.at[t], x_sem.at[n])
         for n, (src, dst) in enumerate(((w_gate, wg), (w_up, wu), (w_down, wdn)))
@@ -166,11 +183,11 @@
     ]
     for copy in small:
         copy.start()
-    for n in range(3):
-        load[n].start()
+    load_start(0)
+    load_start(1)
     for copy in small:
         copy.wait()
-    lax.fori_loop(0, chunks, lambda c, carry: (in_copy(c).start(), carry)[1], 0)
+    load_start(2)
 
     normed = rms_scale(tokens[...].astype(F32), attn_gain[...]).astype(BF16)
 
@@ -206,54 +223,69 @@
     spread[...] = mine.T.astype(BF16)
     picks[...] = jnp.concatenate(found, axis=0).astype(BF16)
 
-    load[0].wait()
+    load_wait(0)
+    for c in range(chunks // 3):
+        in_copy(c).start()
     raw_q = rounded(wbuf[0])
-    load[1].wait()
+    load_wait(1)
+    for c in range(chunks // 3, 2 * chunks // 3):
+        in_copy(c).start()
     raw_k = rounded(wbuf[1])
-    for n in (3, 4):
-        load[n].start()
     for h in range(heads):
         span = slice(h * dim, (h + 1) * dim)
         query = unit_rows(silu(raw_q[:, span])) * dim ** (-0.5)
         key = unit_rows(silu(raw_k[:, span]))
         kq[:, h, :] = key
+        turned[h] = key.T
         kq[:, heads + h, :] = query
         dots[:, h, :] = jnp.broadcast_to(jnp.sum(key * query, axis=-1, keepdims=True), (seqs, dim))
-    load[2].wait()
+    load_wait(2)
+    for c in range(2 * chunks // 3, chunks):
+        in_copy(c).start()
     value = silu(rounded(wbuf[2]))
     for h in range(heads):
         vals[:, h, :] = value[:, h * dim : (h + 1) * dim]
-    for copy in experts:
-        copy.start()
-
-    def one_chunk(c, carry):
+
+    def hits_of(c):
         in_copy(c).wait()
         hits = []
+        for s in range(c * step, (c + 1) * step):
+            lhs = kq[s].astype(BF16)
+            hits.append([jnp.dot(lhs, ns[s, h].astype(BF16), preferred_element_type=F32) for h in range(heads)])
+        return hits
+
+    def update(c, hits):
         for i in range(step):
             s = c * step + i
-            lhs = kq[s].astype(BF16)
-            hits.append([jnp.dot(lhs, ns[s, h].astype(BF16), preferred_element_type=F32) for h in range(heads)])
-        for i in range(step):
-            s = c * step + i
-            turned = kq[s].T
             fs, bs, vs, ds = fades[s], betas[s], vals[s], dots[s]
             for h in range(heads):
                 hit = hits[i][h]
                 f = fs[h : h + 1]
                 written = bs[h : h + 1] * (vs[h : h + 1] - f * hit[h : h + 1])
-                kc = jnp.broadcast_to(turned[:, h : h + 1], (dim, dim))
+                kc = jnp.broadcast_to(turned[h, :, s : s + 1], (dim, dim))
                 ns[s, h] = f * ns[s, h] + kc * written
                 reads[s, pl.ds(h, 1)] = f * hit[heads + h : heads + h + 1] + written * ds[h : h + 1]
-        return carry
-
-    lax.fori_loop(0, chunks, one_chunk, 0)
-    load[3].wait()
+
+    before = None
+    for c in range(chunks):
+        hits = hits_of(c)
+        if c == 0:
+            load_start(3)
+        if c == min(2, chunks - 1):
+            load_start(4)
+        if before is not None:
+            update(c - 1, before)
+        before = hits
+    update(chunks - 1, before)
+    for copy in experts:
+        copy.start()
+    load_wait(3)
     zbuf[...] = silu(rounded(wbuf[3]))
     mixed = []
     for h in range(heads):
         span = slice(h * dim, (h + 1) * dim)
         mixed.append((rms_scale(reads[:, h, :], out_gain[...]) * zbuf[:, span]).astype(BF16))
-    load[4].wait()
+    load_wait(4)
     part_out[...] = jnp.dot(jnp.concatenate(mixed, axis=1), wo[...], preferred_element_type=F32).astype(BF16)
     pl.semaphore_wait(barrier, n_ep)
 
@@ -308,7 +340,7 @@
 
             @pl.when(t == c)
             def _(n=n):
-                lax.fori_loop(0, n_ep - 1, lambda i, carry: (go(n, far(i)).start(), carry)[1], 0)
+                lax.fori_loop(0, n_ep - 1, lambda i, carry: (go(n, across(i)).start(), carry)[1], 0)
 
     arrived[e] = disp[e]
     for n in (1, 2):
@@ -342,7 +374,7 @@
             def _(n=n, c=c):
                 def send(i, carry):
                     for d in range(n_tp):
-                        back(n, d, far(i)).start()
+                        back(n, d, rising(i)).start()
                     return carry
 
                 lax.fori_loop(0, n_ep - 1, send, 0)
@@ -380,6 +412,17 @@
                 all_go(n, 0).wait()
                 for d in range(n_tp):
                     all_back(n, d, n_ep - 1 + d, back_sem.at[0]).wait()
+
+
+def flush_kernel(step, out_ref, ns_ref, out, ns, sem):
+    copies = [pltpu.make_async_copy(out_ref, out, sem.at[0])]
+    for s in range(0, ns.shape[0], step):
+        rows = pl.ds(s, step)
+        copies.append(pltpu.make_async_copy(ns_ref.at[rows], ns.at[rows], sem.at[1]))
+    for copy in copies:
+        copy.start()
+    copies[0].wait()
+    pltpu.make_async_copy(ns_ref, ns, sem.at[1]).wait()
 
 
 def per_device(
@@ -420,7 +463,7 @@
     slots = n_ep * cap
     vmem = pltpu.VMEM
     dma = pltpu.SemaphoreType.DMA
-    return pl.pallas_call(
+    layer_out, new_state = pl.pallas_call(
         functools.partial(layer_kernel, n_ep, n_tp, top, cap, shares, step),
         out_shape=(vmem((seqs, cols), BF16), vmem(state.shape, F32)),
         in_specs=[HBM] * 19,
@@ -447,6 +490,7 @@
             vmem((seqs, heads, dim), F32),
             vmem((seqs, heads, dim), F32),
             vmem((seqs, heads, dim), F32),
+            vmem((heads, dim, seqs), F32),
             vmem((seqs, heads, dim), F32),
             vmem((slots, seqs), BF16),
             vmem((top * seqs, n_tp * slots), BF16),
@@ -492,6 +536,18 @@
         expert_up,
         expert_down,
     )
+    return pl.pallas_call(
+        functools.partial(flush_kernel, step),
+        out_shape=(jax.ShapeDtypeStruct((seqs, cols), BF16), jax.ShapeDtypeStruct(state.shape, F32)),
+        in_specs=[VMEM, VMEM],
+        out_specs=(HBM, HBM),
+        scratch_shapes=[dma((2,))],
+        compiler_params=pltpu.CompilerParams(vmem_limit_bytes=2**20),
+        name="flush",
+    )(
+        pltpu.with_memory_space_constraint(layer_out, pltpu.VMEM),
+        pltpu.with_memory_space_constraint(new_state, pltpu.VMEM),
+    )
 
 
 def solution(mesh):

time: 42.6 us -> 28.4 us (0.67)
  local copies, waits for them, and re-layouts: 14 us -> 0 us
    unnamed x28 -> x0, local copies, waits for them, and re-layouts: 14 us -> none
    pallas_call x0 -> x1, Pallas kernels: none -> 2.7 us  [per_device(): pl.pallas_call(functools.partial(flush_kernel, step), out_shape=(jax.Shap...]
    pallas_call x1, Pallas kernels: 27.4 us -> 24.9 us  [per_device(): pl.pallas_call(functools.partial(layer_kernel, n_ep, n_tp, top, cap, shar...]
where the time goes in v2:
time: 28.4 us; the launch traced here: 28.2 us
  Pallas kernels  27.6 us (97%)
  between operations  0.65 us (2%)
    pallas_call x1, Pallas kernels, per_device(): pl.pallas_call(functools.partial(layer_kernel, n_ep, n_tp, top, cap, shar...  24.9 us
    pallas_call x1, Pallas kernels, per_device(): pl.pallas_call(functools.partial(flush_kernel, step), out_shape=(jax.Shap...  2.7 us

profile of v2, /device:TPU:0, one launch (start us, length us, event | category | flops | bytes accessed | tf_op | source)
XLA Modules:
  0.0 28.2 jit_solution(4364075217794727751)
XLA Ops:
  0.6 24.9 %layer.1 = (bf16[24,1024]{1,0:T(8,128)(2,1)S(1)}, f32[24,4,128,128]{3,2,1,0:T(8,128)S(1)}) custom-call(bf16[24,2048]{1,0:T(8,128)(2,1)} %tokens_ref.1, f32[1,2048]{1,0:T(1,128)} %bitcast.11, bf16[4,2048]{1,0:T(4,128)(2,1)} %bitcast.9, bf16[4,2048]{1,0:T(4,128)(2,1)} %bitcast.10, f32[1,4]{1,0:T(1,128)} %bitcast.15, f32[1,4]{1,0:T(1,128)} %bitcast.16, ...), custom_call_target="tpu_custom_call" | custom-call | tf_op jit(solution)/shard_map/layer/pallas_call | solution.py:466
  25.5 2.7 %flush.1 = (bf16[24,1024]{1,0:T(8,128)(2,1)}, f32[24,4,128,128]{3,2,1,0:T(8,128)}) custom-call(bf16[24,1024]{1,0:T(8,128)(2,1)S(1)} %get-tuple-element.4.out_ref, f32[24,4,128,128]{3,2,1,0:T(8,128)S(1)} %get-tuple-element.5.ns_ref), custom_call_target="tpu_custom_call" | custom-call | tf_op jit(solution)/shard_map/flush/pallas_call | solution.py:539

commit v3 on v2

--- a/solution.py
+++ b/solution.py
@@ -10,6 +10,7 @@
 EPS = 1e-06
 F32 = jnp.float32
 BF16 = jnp.bfloat16
+CUTS = (6,)
 VMEM_LIMIT = 57 * 1024 * 1024
 HBM = pl.BlockSpec(memory_space=pltpu.HBM)
 VMEM = pl.BlockSpec(memory_space=pltpu.VMEM)
@@ -42,6 +43,8 @@
     cap,
     shares,
     step,
+    order,
+    bounds,
     tokens_ref,
     attn_ref,
     wd_ref,
@@ -117,22 +120,18 @@
     barrier = pltpu.get_barrier_semaphore()
     pl.semaphore_signal(barrier, inc=1, device_id=partner, device_id_type=mesh_ids)
 
-    bits = [1 << b for b in range((n_ep - 1).bit_length())] if n_ep & (n_ep - 1) == 0 else []
-    flips = [bit * (1 - 2 * lax.rem(e // bit, 2)) for bit in bits]
-
-    def across(i):
-        if not bits:
-            return lax.rem(e + 1 + i, n_ep)
-        p = e
-        for bit, flip in zip(bits, flips):
-            p = p + flip * lax.rem((n_ep - 1 - i) // bit, 2)
-        return p
-
-    def rising(i):
-        return lax.rem(i + jnp.where(i >= e, 1, 0), n_ep)
+    groups = len(bounds) - 1
+    rank = sum((jnp.where(e == p, k, 0) for k, p in enumerate(order)), 0)
+    mine_group = sum((jnp.where(rank >= b, 1, 0) for b in bounds[1:-1]), 0)
+    bits = [1 << k for k in range((n_ep - 1).bit_length())] if n_ep & (n_ep - 1) == 0 else []
+    flips = [(b, b * (1 - 2 * lax.rem(e // b, 2))) for b in bits]
+
+    def peer(i):
+        return sum((flip for b, flip in flips if (n_ep - i) & b), e) if bits else lax.rem(e + i, n_ep)
 
     def greet(i, carry):
-        pl.semaphore_signal(barrier, inc=1, device_id={"ep": rising(i), "tp": t}, device_id_type=mesh_ids)
+        p = lax.rem(e + 1 + i, n_ep)
+        pl.semaphore_signal(barrier, inc=1, device_id={"ep": p, "tp": t}, device_id_type=mesh_ids)
         return carry
 
     lax.fori_loop(0, n_ep - 1, greet, 0)
@@ -240,6 +239,7 @@
         kq[:, heads + h, :] = query
         dots[:, h, :] = jnp.broadcast_to(jnp.sum(key * query, axis=-1, keepdims=True), (seqs, dim))
     load_wait(2)
+    load_start(3)
     for c in range(2 * chunks // 3, chunks):
         in_copy(c).start()
     value = silu(rounded(wbuf[2]))
@@ -267,20 +267,22 @@
                 reads[s, pl.ds(h, 1)] = f * hit[heads + h : heads + h + 1] + written * ds[h : h + 1]
 
     before = None
+    zc = max(chunks - 2, 0)
     for c in range(chunks):
         hits = hits_of(c)
-        if c == 0:
-            load_start(3)
-        if c == min(2, chunks - 1):
+        if c == min(1, chunks - 1):
             load_start(4)
+        if c == chunks - 1:
+            experts[0].start()
+        if c == zc:
+            load_wait(3)
+            zbuf[...] = silu(rounded(wbuf[3]))
         if before is not None:
             update(c - 1, before)
         before = hits
     update(chunks - 1, before)
-    for copy in experts:
+    for copy in experts[1:]:
         copy.start()
-    load_wait(3)
-    zbuf[...] = silu(rounded(wbuf[3]))
     mixed = []
     for h in range(heads):
         span = slice(h * dim, (h + 1) * dim)
@@ -300,7 +302,7 @@
     swap.start()
     experts[0].wait()
     push[0].start()
-    swap.wait()
+    swap.wait_recv()
     rows = tokens[...].astype(F32) + (part_out[...].astype(F32) + part_in[...].astype(F32))
     resid[...] = rows
     moe = rms_scale(rows, ffn_gain[...]).astype(BF16)
@@ -310,24 +312,24 @@
     def go(n, p):
         return pltpu.make_async_remote_copy(
             src_ref=disp.at[p, pl.ds(0, n)],
-            dst_ref=arrived.at[e, pl.ds(0, n)],
-            send_sem=go_sem.at[0],
-            recv_sem=go_sem.at[1],
+            dst_ref=arrived.at[rank, pl.ds(0, n)],
+            send_sem=go_sem.at[groups],
+            recv_sem=go_sem.at[mine_group],
             device_id={"ep": p, "tp": t},
             device_id_type=mesh_ids,
         )
 
-    def all_go(n, which):
-        block = arrived.at[pl.ds(0, n_ep - 1), pl.ds(0, n)]
+    def all_go(n, count, which):
+        block = arrived.at[pl.ds(0, count), pl.ds(0, n)]
         return pltpu.make_async_copy(block, block, go_sem.at[which])
 
-    def back(n, c, p):
+    def back(n, c, k):
         return pltpu.make_async_remote_copy(
-            src_ref=ret_out.at[c, p, pl.ds(0, n)],
+            src_ref=ret_out.at[c, k, pl.ds(0, n)],
             dst_ref=ret_in.at[t, e, pl.ds(0, n)],
             send_sem=back_sem.at[0],
             recv_sem=back_recv.at[t],
-            device_id={"ep": p, "tp": c},
+            device_id={"ep": order[k], "tp": c},
             device_id_type=mesh_ids,
         )
 
@@ -340,49 +342,60 @@
 
             @pl.when(t == c)
             def _(n=n):
-                lax.fori_loop(0, n_ep - 1, lambda i, carry: (go(n, across(i)).start(), carry)[1], 0)
-
-    arrived[e] = disp[e]
+                for i in range(1, n_ep):
+                    go(n, peer(i)).start()
+
+    arrived[rank] = disp[e]
     for n in (1, 2):
         experts[n].wait()
         push[n].start()
-    for c, n in enumerate(shares):
-        if n:
-
-            @pl.when(t == c)
-            def _(n=n):
-                all_go(n, 1).wait()
-
-    got = arrived[...].astype(F32).reshape(slots, width).astype(BF16)
-    push[0].wait_recv()
-    gates = [jnp.dot(got, wg[h], preferred_element_type=F32) for h in range(n_tp)]
-    push[1].wait_recv()
-    ups = [jnp.dot(got, wu[h], preferred_element_type=F32) for h in range(n_tp)]
-    hidden = [(silu(gates[h]) * ups[h]).astype(BF16) for h in range(n_tp)]
-    push[2].wait_recv()
-    for c in range(n_tp):
-        term = None
-        for h in range(n_tp):
-            piece = jnp.dot(hidden[h], wdn[h, :, c * cols : (c + 1) * cols], preferred_element_type=F32)
-            term = piece if term is None else term + piece
-        ret_out[c] = term.reshape(n_ep, cap, cols).astype(BF16)
-
-    for c, n in enumerate(shares):
-        if n:
-
-            @pl.when(t == c)
-            def _(n=n, c=c):
-                def send(i, carry):
-                    for d in range(n_tp):
-                        back(n, d, rising(i)).start()
-                    return carry
-
-                lax.fori_loop(0, n_ep - 1, send, 0)
-                for d in range(n_tp):
-                    if d != c:
-                        back(n, d, e).start()
-
-    ret_in[t, e] = ret_out[t, e]
+    for g in range(groups):
+        low, high = bounds[g], bounds[g + 1]
+        size = high - low
+        span = pl.ds(low, size)
+        for c, n in enumerate(shares):
+            if n:
+
+                @pl.when((t == c) & (mine_group == g))
+                def _(n=n, g=g, size=size):
+                    if size > 1:
+                        all_go(n, size - 1, g).wait()
+
+                @pl.when((t == c) & (mine_group != g))
+                def _(n=n, g=g, size=size):
+                    all_go(n, size, g).wait()
+
+        got = arrived[span].astype(F32).reshape(size * cap, width).astype(BF16)
+        if g == 0:
+            push[0].wait_recv()
+        gates = [jnp.dot(got, wg[h], preferred_element_type=F32) for h in range(n_tp)]
+        if g == 0:
+            push[1].wait_recv()
+        ups = [jnp.dot(got, wu[h], preferred_element_type=F32) for h in range(n_tp)]
+        hidden = [(silu(gates[h]) * ups[h]).astype(BF16) for h in range(n_tp)]
+        if g == 0:
+            push[2].wait_recv()
+        for d in range(n_tp):
+            term = None
+            for h in range(n_tp):
+                piece = jnp.dot(hidden[h], wdn[h, :, d * cols : (d + 1) * cols], preferred_element_type=F32)
+                term = piece if term is None else term + piece
+            ret_out[d, span] = term.reshape(size, cap, cols).astype(BF16)
+            for c, n in enumerate(shares):
+                if n:
+
+                    @pl.when(t == c)
+                    def _(n=n, c=c, d=d, low=low, high=high):
+                        for k in range(low, high):
+                            if d != c:
+                                back(n, d, k).start()
+                            else:
+
+                                @pl.when(e != order[k])
+                                def _(k=k):
+                                    back(n, d, k).start()
+
+    ret_in[t, e] = ret_out[t, rank]
     total = resid[:, pl.ds(pl.multiple_of(t * cols, 128), cols)]
     scale = [column(weights[j : j + 1, :]) for j in range(top)]
     for c, n in enumerate(shares):
@@ -402,14 +415,14 @@
         total = total + combined[j * seqs : (j + 1) * seqs] * scale[j]
     out[...] = total.astype(BF16)
 
-    for copy in push:
+    for copy in (swap, *push):
         copy.wait_send()
     for c, n in enumerate(shares):
         if n:
 
             @pl.when(t == c)
             def _(n=n):
-                all_go(n, 0).wait()
+                all_go(n, n_ep - 1, groups).wait()
                 for d in range(n_tp):
                     all_back(n, d, n_ep - 1 + d, back_sem.at[0]).wait()
 
@@ -428,6 +441,7 @@
 def per_device(
     n_ep,
     n_tp,
+    order,
     tokens,
     attn_gain,
     w_query,
@@ -455,16 +469,18 @@
     step = 4 if seqs % 4 == 0 else 1
     chunks = seqs // step
     live = max(2, 2 * seqs * top // n_ep)
-    first = 2 * -(-live // 4)
-    shares = (first, live - first)
-    cap = -(-first // 8) * 8
+    most = 2 * -(-live // 4)
+    shares = (live - most, most)
+    cap = -(-most // 8) * 8
+    bounds = sorted({0, n_ep, *(n_ep * share // 16 for share in CUTS)})
+    groups = len(bounds) - 1
     cols = width // n_tp
     ff = expert_gate.shape[2]
     slots = n_ep * cap
     vmem = pltpu.VMEM
     dma = pltpu.SemaphoreType.DMA
     layer_out, new_state = pl.pallas_call(
-        functools.partial(layer_kernel, n_ep, n_tp, top, cap, shares, step),
+        functools.partial(layer_kernel, n_ep, n_tp, top, cap, shares, step, order, bounds),
         out_shape=(vmem((seqs, cols), BF16), vmem(state.shape, F32)),
         in_specs=[HBM] * 19,
         out_specs=(VMEM, VMEM),
@@ -507,7 +523,7 @@
             dma((3,)),
             dma((2,)),
             dma((2, 3)),
-            dma((2,)),
+            dma((groups + 1,)),
             dma((1,)),
             dma((n_tp,)),
         ],
@@ -573,5 +589,8 @@
         P("ep", None),
     )
     out_specs = (P("ep", "tp"), P("ep", "tp", None, None))
-    body = functools.partial(per_device, mesh.shape["ep"], mesh.shape["tp"])
+    n_ep, n_tp = mesh.shape["ep"], mesh.shape["tp"]
+    chips = mesh.devices.reshape(n_ep, n_tp)[:, 0]
+    order = sorted(range(n_ep), key=lambda p: sum(getattr(chips[p], "coords", (p,))))
+    body = functools.partial(per_device, n_ep, n_tp, order)
     return jax.shard_map(body, mesh=mesh, in_specs=in_specs, out_specs=out_specs, check_vma=False)

time: 28.4 us -> 27.3 us (0.961)
  Pallas kernels: 27.6 us -> 26.4 us
    pallas_call x1, Pallas kernels: 24.9 us -> 23.7 us  [per_device(): pl.pallas_call(functools.partial(layer_kernel, n_ep, n_tp, top, cap, shar...]
where the time goes in v3:
time: 27.3 us; the launch traced here: 27.1 us
  Pallas kernels  26.4 us (97%)
  between operations  0.65 us (2%)
    pallas_call x1, Pallas kernels, per_device(): pl.pallas_call(functools.partial(layer_kernel, n_ep, n_tp, top, cap, shar...  23.7 us
    pallas_call x1, Pallas kernels, per_device(): pl.pallas_call(functools.partial(flush_kernel, step), out_shape=(jax.Shap...  2.7 us

profile of v3, /device:TPU:0, one launch (start us, length us, event | category | flops | bytes accessed | tf_op | source)
XLA Modules:
  0.0 27.1 jit_solution(2770961199592061654)
XLA Ops:
  0.6 23.7 %layer.1 = (bf16[24,1024]{1,0:T(8,128)(2,1)S(1)}, f32[24,4,128,128]{3,2,1,0:T(8,128)S(1)}) custom-call(bf16[24,2048]{1,0:T(8,128)(2,1)} %tokens_ref.1, f32[1,2048]{1,0:T(1,128)} %bitcast.11, bf16[4,2048]{1,0:T(4,128)(2,1)} %bitcast.9, bf16[4,2048]{1,0:T(4,128)(2,1)} %bitcast.10, f32[1,4]{1,0:T(1,128)} %bitcast.15, f32[1,4]{1,0:T(1,128)} %bitcast.16, ...), custom_call_target="tpu_custom_call" | custom-call | tf_op jit(solution)/shard_map/layer/pallas_call | solution.py:482
  24.4 2.7 %flush.1 = (bf16[24,1024]{1,0:T(8,128)(2,1)}, f32[24,4,128,128]{3,2,1,0:T(8,128)}) custom-call(bf16[24,1024]{1,0:T(8,128)(2,1)S(1)} %get-tuple-element.4.out_ref, f32[24,4,128,128]{3,2,1,0:T(8,128)S(1)} %get-tuple-element.5.ns_ref), custom_call_target="tpu_custom_call" | custom-call | tf_op jit(solution)/shard_map/flush/pallas_call | solution.py:555

commit v4 on v3

--- a/solution.py
+++ b/solution.py
@@ -10,7 +10,7 @@
 EPS = 1e-06
 F32 = jnp.float32
 BF16 = jnp.bfloat16
-CUTS = (6,)
+CUTS = (4,)
 VMEM_LIMIT = 57 * 1024 * 1024
 HBM = pl.BlockSpec(memory_space=pltpu.HBM)
 VMEM = pl.BlockSpec(memory_space=pltpu.VMEM)

time: 27.3 us -> 26.9 us (0.985)
  the two profiles are of different devices: /device:TPU:0 before, /device:TPU:25 now
where the time goes in v4:
time: 26.9 us; the launch traced here: 26.8 us
  Pallas kernels  26.1 us (97%)
  between operations  0.65 us (2%)
    pallas_call x1, Pallas kernels, per_device(): pl.pallas_call(functools.partial(layer_kernel, n_ep, n_tp, top, cap, shar...  23.4 us
    pallas_call x1, Pallas kernels, per_device(): pl.pallas_call(functools.partial(flush_kernel, step), out_shape=(jax.Shap...  2.7 us

profile of v4, /device:TPU:25, one launch (start us, length us, event | category | flops | bytes accessed | tf_op | source)
XLA Modules:
  0.0 26.8 jit_solution(9837343637862652592)
XLA Ops:
  0.6 23.4 %layer.1 = (bf16[24,1024]{1,0:T(8,128)(2,1)S(1)}, f32[24,4,128,128]{3,2,1,0:T(8,128)S(1)}) custom-call(bf16[24,2048]{1,0:T(8,128)(2,1)} %tokens_ref.1, f32[1,2048]{1,0:T(1,128)} %bitcast.11, bf16[4,2048]{1,0:T(4,128)(2,1)} %bitcast.9, bf16[4,2048]{1,0:T(4,128)(2,1)} %bitcast.10, f32[1,4]{1,0:T(1,128)} %bitcast.15, f32[1,4]{1,0:T(1,128)} %bitcast.16, ...), custom_call_target="tpu_custom_call" | custom-call | tf_op jit(solution)/shard_map/layer/pallas_call | solution.py:482
  24.1 2.7 %flush.1 = (bf16[24,1024]{1,0:T(8,128)(2,1)}, f32[24,4,128,128]{3,2,1,0:T(8,128)}) custom-call(bf16[24,1024]{1,0:T(8,128)(2,1)S(1)} %get-tuple-element.4.out_ref, f32[24,4,128,128]{3,2,1,0:T(8,128)S(1)} %get-tuple-element.5.ns_ref), custom_call_target="tpu_custom_call" | custom-call | tf_op jit(solution)/shard_map/flush/pallas_call | solution.py:555
